TPU v7x, 32 devices: a whole 2x2x4 slice. The times are simulated.
32 devices in a mesh: sp: 16 (over z, y, x), tp: 2 (over core).
Axes of the slice: x: 2, y: 2, z: 4, core: 2. Of those that a mesh axis runs over, the one named last changes fastest.
Arguments:
- residual: bfloat16 [4096, 2048], P(('sp', 'tp')), may hold values from -6 to 6
- projected: bfloat16 [4096, 2048], P('sp', 'tp'), may hold values from -6 to 6
- group_weight: bfloat16 [4, 512, 512], P('tp'), may hold values from -0.25 to 0.25
- channel_scale: float32 [2048], P('tp'), may hold values from 0.1 to 1.9
- out_weight: bfloat16 [2048, 2048], replicated, may hold values from -0.125 to 0.125
- post_mix_gain: float32 [2048], replicated, may hold values from 0.1 to 1.9
- pre_ffn_gain: float32 [2048], replicated, may hold values from 0.1 to 1.9
- post_ffn_gain: float32 [2048], replicated, may hold values from 0.1 to 1.9
- route_ids: int32 [4096, 2], P(('sp', 'tp')), may hold values from 0 to 7, all different within a row; in each aligned block of 128 rows (0 to 127, 128 to 255, ...) at most 64 rows name the same one
- route_weight: float32 [4096, 2], P(('sp', 'tp')), may hold values from 0.1 to 1
- expert_gate: bfloat16 [16, 2048, 1792], P('sp', None, 'tp'), may hold values from -0.125 to 0.125
- expert_up: bfloat16 [16, 2048, 1792], P('sp', None, 'tp'), may hold values from -0.125 to 0.125
- expert_down: bfloat16 [16, 1792, 2048], P('sp', 'tp'), may hold values from -0.09375 to 0.09375
Outputs:
- layer_out: bfloat16 [4096, 2048], P(('sp', 'tp'))
Inputs may be any that keep to these rules, and one draw needn't show every extreme that they name: `route_ids`: each row names 2 different experts. In every aligned block of 128 rows (the rows of one device) no expert is named more than 64 times, a bound that some blocks reach.
All inputs are finite; a program needn't handle non-finite values.
Results may differ from a plain program's by a relative error of at most 0.014.
Values may be sent and summed in bfloat16 or wider, within the bound.
A program may use at most 192 MiB of HBM per device.

v0:
```python
import functools

import jax
import jax.numpy as jnp
from jax import lax
from jax.experimental import pallas as pl
from jax.experimental.pallas import tpu as pltpu
from jax.sharding import PartitionSpec as P

GROUPS = 4
TOP = 2


EPS = 1e-06
MESH = pl.DeviceIdType.MESH
TILE = 256
WIDE = 512
GROUP_ROWS = 256


def rms_scale(values, gain):
    inverse = lax.rsqrt(jnp.mean(values * values, axis=-1, keepdims=True) + EPS)
    return values * inverse * gain


def flipped(index, mask, count):
    result = 0
    bit = 1
    while bit < count:
        digit = (index // bit) % 2
        result = result + (1 - digit if mask & bit else digit) * bit
        bit = bit * 2
    return result


def layer_kernel(
    experts,
    cap,
    residual,
    projected,
    group_weight,
    channel_scale,
    out_hbm,
    post_mix_gain,
    pre_ffn_gain,
    post_ffn_gain,
    route_ids,
    route_weight,
    gate_hbm,
    up_hbm,
    down_hbm,
    result,
    gate_all,
    up_all,
    down_all,
    rows,
    active,
    partial,
    mirrored,
    table,
    back,
    out_all,
    halo,
    scaled,
    received,
    mixed,
    middle,
    local_sem,
    weight_send,
    weight_recv,
    out_send,
    out_recv,
    twin_send,
    twin_recv,
    swap_send,
    swap_recv,
    back_send,
    back_recv,
    front_send,
    front_recv,
):
    place = lax.axis_index("sp")
    core = lax.axis_index("tp")
    expert, side = place // 2, place % 2
    twin = (place + 1 - 2 * side, core)
    partner = (place, 1 - core)
    peers = [None] + [(2 * flipped(expert, r, experts) + side, core) for r in range(1, experts)]
    quarter = gate_hbm.shape[2]
    hidden = 2 * quarter
    width = residual.shape[1]
    half_rows = GROUP_ROWS // 2
    per_group = half_rows // cap
    places = lax.axis_size("sp")
    tokens = projected.shape[0]
    share = tokens // 2
    cut = projected.shape[1]
    lookback = halo.shape[0]
    groups = experts // per_group

    def spot(r, mirror):
        return (r // per_group) * GROUP_ROWS + mirror * half_rows + (r % per_group) * cap

    def send(source, target, device, first, second):
        copy = pltpu.make_async_remote_copy(
            src_ref=source,
            dst_ref=target,
            send_sem=first,
            recv_sem=second,
            device_id=device,
            device_id_type=MESH,
        )
        copy.start()
        return copy

    weights = [
        (gate_hbm.at[0], gate_all.at[:, pl.ds(0, quarter)], gate_all.at[:, pl.ds(quarter, quarter)]),
        (up_hbm.at[0], up_all.at[:, pl.ds(0, quarter)], up_all.at[:, pl.ds(quarter, quarter)]),
        (down_hbm.at[0], down_all.at[pl.ds(0, quarter)], down_all.at[pl.ds(quarter, quarter)]),
    ]
    out_load = pltpu.make_async_copy(out_hbm, out_all, local_sem.at[3])
    out_load.start()
    loads = []
    for i, (source, own, _) in enumerate(weights):
        load = pltpu.make_async_copy(source, own, local_sem.at[i])
        load.start()
        loads.append(load)

    barrier = pltpu.get_barrier_semaphore()
    ring = [((place + 1) % places, core), ((place + places - 1) % places, core)]
    for device in peers[1:] + [twin, partner] + ring:
        pl.semaphore_signal(barrier, inc=1, device_id=device, device_id_type=MESH)
    pl.semaphore_wait(barrier, experts + 3)

    edge = pltpu.make_async_remote_copy(
        src_ref=projected.at[pl.ds(tokens - lookback, lookback)],
        dst_ref=halo,
        send_sem=front_send.at[0],
        recv_sem=front_recv.at[0],
        device_id=ring[0],
        device_id_type=MESH,
    )

    @pl.when(place < places - 1)
    def _():
        edge.start()

    columns = lax.broadcasted_iota(jnp.int32, (share, experts * cap), 1)
    owner = (columns // cap) ^ expert
    named = [owner == route_ids[:, k : k + 1] for k in range(TOP)]
    member = functools.reduce(jnp.logical_or, named).astype(jnp.float32)
    earlier = (
        lax.broadcasted_iota(jnp.int32, (share, share), 1)
        < lax.broadcasted_iota(jnp.int32, (share, share), 0)
    ).astype(jnp.bfloat16)
    rank = jnp.dot(earlier, member.astype(jnp.bfloat16), preferred_element_type=jnp.float32)
    chosen = jnp.where(rank == (columns % cap).astype(jnp.float32), member, 0.0)
    spread = chosen.T.astype(jnp.bfloat16)
    picks = [jnp.where(hit, chosen, 0.0).astype(jnp.bfloat16) for hit in named]

    @pl.when(place > 0)
    def _():
        edge.wait_recv()

    @pl.when(place == 0)
    def _():
        halo[...] = jnp.zeros_like(halo)

    position = (
        place * tokens + lax.broadcasted_iota(jnp.int32, (tokens, 1), 0) + 1
    ).astype(jnp.float32)
    groups_here = group_weight.shape[0]
    group_width = cut // groups_here
    for local_group in range(groups_here):
        low = local_group * group_width
        own_part = projected[:, low : low + group_width].astype(jnp.float32)
        current = jnp.concatenate(
            [halo[:, low : low + group_width].astype(jnp.float32), own_part], 0
        )
        group_id = core * groups_here + local_group
        summed = own_part
        window_span = jnp.float32(1.0)
        for level_id in range(GROUPS):
            current = current + pltpu.roll(current, 2**level_id, 0)
            hit = group_id == level_id
            summed = jnp.where(hit, current[lookback:], summed)
            window_span = jnp.where(hit, jnp.float32(2.0 ** (level_id + 1)), window_span)
        pooled = (summed / jnp.minimum(position, window_span) - own_part).astype(jnp.bfloat16)
        grouped = jnp.dot(pooled, group_weight[local_group], preferred_element_type=jnp.float32)
        scaled[:, low : low + group_width] = (
            grouped * channel_scale[:, low : low + group_width]
        ).astype(jnp.bfloat16)
    there = pl.ds(pl.multiple_of((1 - core) * share, share), share)
    here = pl.ds(pl.multiple_of(core * share, share), share)
    exchange = send(scaled.at[there], received, partner, front_send.at[1], front_recv.at[1])
    out_load.wait()

    def mix(block, first_row, fresh):
        def step(t, carry):
            at = pl.ds(pl.multiple_of(t * WIDE, WIDE), WIDE)
            value = jnp.dot(
                block, out_all[pl.ds(first_row, cut), at], preferred_element_type=jnp.float32
            )
            mixed[:, at] = value if fresh else mixed[:, at] + value
            return carry

        lax.fori_loop(0, width // WIDE, step, 0)

    mix(scaled[here], pl.multiple_of(core * cut, cut), True)
    exchange.wait_recv()
    gathers = [
        send(source, theirs, partner, weight_send.at[i], weight_recv.at[i])
        for i, (source, _, theirs) in enumerate(weights)
    ]
    mix(received[...], pl.multiple_of((1 - core) * cut, cut), False)
    rounded = mixed[...].astype(jnp.bfloat16).astype(jnp.float32)
    kept = residual[...].astype(jnp.float32) + rms_scale(rounded, post_mix_gain[...])
    middle[...] = kept.astype(jnp.bfloat16)
    normed = rms_scale(middle[...].astype(jnp.float32), pre_ffn_gain[...]).astype(jnp.bfloat16)
    for low in range(0, width, WIDE):
        block = jnp.dot(spread, normed[:, low : low + WIDE], preferred_element_type=jnp.float32)
        table[:, :, low : low + WIDE] = block.astype(jnp.bfloat16).reshape(experts, cap, WIDE)
    rows[pl.ds(spot(0, 0), cap)] = table[0]

    outs = [None] + [
        send(
            table.at[r],
            rows.at[pl.ds(spot(r, 0), cap)],
            peers[r],
            out_send.at[r],
            out_recv.at[r],
        )
        for r in range(1, experts)
    ]
    twins = [None] * experts
    twins[0] = send(
        table.at[0], rows.at[pl.ds(spot(0, 1), cap)], twin, twin_send.at[0], twin_recv.at[0]
    )
    swaps = [None] * experts
    backs = [None] * experts

    def forward(g):
        for r in range(g * per_group, (g + 1) * per_group):
            if r > 0:
                outs[r].wait_recv()
                twins[r] = send(
                    rows.at[pl.ds(spot(r, 0), cap)],
                    rows.at[pl.ds(spot(r, 1), cap)],
                    twin,
                    twin_send.at[r],
                    twin_recv.at[r],
                )

    def compute(g):
        base = g * GROUP_ROWS
        for r in range(g * per_group, (g + 1) * per_group):
            twins[r].wait_recv()
        if g == 0:
            for i in range(2):
                loads[i].wait()
                gathers[i].wait_recv()

        def enter(t, carry):
            at = pl.ds(pl.multiple_of(t * TILE, TILE), TILE)
            here = rows[pl.ds(base, GROUP_ROWS), :]
            gate = jnp.dot(here, gate_all[:, at], preferred_element_type=jnp.float32)
            up = jnp.dot(here, up_all[:, at], preferred_element_type=jnp.float32)
            active[:, at] = (jax.nn.silu(gate) * up).astype(jnp.bfloat16)
            return carry

        lax.fori_loop(0, hidden // TILE, enter, 0)
        if g == 0:
            loads[2].wait()
            gathers[2].wait_recv()

        def leave(t, carry):
            at = pl.ds(pl.multiple_of(t * TILE, TILE), TILE)
            value = jnp.dot(active[...], down_all[:, at], preferred_element_type=jnp.float32)
            partial[pl.ds(base, GROUP_ROWS), at] = value.astype(jnp.bfloat16)
            return carry

        lax.fori_loop(0, width // TILE, leave, 0)

    def swap(g):
        for r in range(g * per_group, (g + 1) * per_group):
            swaps[r] = send(
                partial.at[pl.ds(spot(r, 1), cap)],
                mirrored.at[r],
                twin,
                swap_send.at[r],
                swap_recv.at[r],
            )

    def finish(g):
        for r in range(g * per_group, (g + 1) * per_group):
            piece = pl.ds(spot(r, 0), cap)
            swaps[r].wait_recv()
            total = partial[piece].astype(jnp.float32) + mirrored[r].astype(jnp.float32)
            partial[piece] = total.astype(jnp.bfloat16)
            if r > 0:
                backs[r] = send(
                    partial.at[piece], back.at[r], peers[r], back_send.at[r], back_recv.at[r]
                )
            else:
                back[0] = partial[piece]

    forward(0)
    forward(1)
    compute(0)
    forward(2)
    swap(0)
    compute(2)
    swap(2)
    forward(3)
    compute(1)
    swap(1)
    finish(0)
    finish(2)
    compute(3)
    swap(3)
    finish(1)
    finish(3)
    for r in range(1, experts):
        backs[r].wait_recv()
    flat = back[...].reshape(experts * cap, width)
    for low in range(0, width, WIDE):
        total = jnp.zeros((share, WIDE), jnp.float32)
        for k in range(TOP):
            picked = jnp.dot(
                picks[k], flat[:, low : low + WIDE], preferred_element_type=jnp.float32
            )
            total = total + picked * route_weight[:, k : k + 1]
        mixed[:, low : low + WIDE] = total
    result[...] = (
        middle[...].astype(jnp.float32) + rms_scale(mixed[...], post_ffn_gain[...])
    ).astype(jnp.bfloat16)
    for r in range(1, experts):
        backs[r].wait_send()
        outs[r].wait_send()
    for copy in twins + swaps + gathers + [exchange]:
        copy.wait_send()

    @pl.when(place < places - 1)
    def _():
        edge.wait_send()


def body(
    residual,
    projected,
    group_weight,
    channel_scale,
    out_weight,
    post_mix_gain,
    pre_ffn_gain,
    post_ffn_gain,
    route_ids,
    route_weight,
    expert_gate,
    expert_up,
    expert_down,
):
    share, width = residual.shape
    tokens, cut = projected.shape
    experts = lax.axis_size("sp") // 2
    cap = 2 * TOP * share // experts
    quarter = expert_gate.shape[2]
    kinds = jnp.bfloat16
    dma = pltpu.SemaphoreType.DMA
    vmem = pl.BlockSpec(memory_space=pltpu.VMEM)
    hbm = pl.BlockSpec(memory_space=pltpu.HBM)
    return pl.pallas_call(
        functools.partial(layer_kernel, experts, cap),
        out_shape=jax.ShapeDtypeStruct((share, width), kinds),
        in_specs=[vmem] * 4 + [hbm] + [vmem] * 5 + [hbm] * 3,
        out_specs=vmem,
        scratch_shapes=[
            pltpu.VMEM((width, 2 * quarter), kinds),
            pltpu.VMEM((width, 2 * quarter), kinds),
            pltpu.VMEM((2 * quarter, width), kinds),
            pltpu.VMEM((2 * experts * cap, width), kinds),
            pltpu.VMEM((GROUP_ROWS, 2 * quarter), kinds),
            pltpu.VMEM((2 * experts * cap, width), kinds),
            pltpu.VMEM((experts, cap, width), kinds),
            pltpu.VMEM((experts, cap, width), kinds),
            pltpu.VMEM((experts, cap, width), kinds),
            pltpu.VMEM(out_weight.shape, kinds),
            pltpu.VMEM((2**GROUPS, cut), kinds),
            pltpu.VMEM((tokens, cut), kinds),
            pltpu.VMEM((share, cut), kinds),
            pltpu.VMEM((share, width), jnp.float32),
            pltpu.VMEM((share, width), kinds),
            dma((4,)),
            dma((3,)),
            dma((3,)),
        ]
        + [dma((experts,))] * 8
        + [dma((2,))] * 2,
        compiler_params=pltpu.CompilerParams(
            collective_id=0, has_side_effects=True, vmem_limit_bytes=62 * 1024 * 1024
        ),
    )(
        residual,
        projected,
        group_weight,
        channel_scale.reshape(1, cut),
        out_weight,
        post_mix_gain.reshape(1, width),
        pre_ffn_gain.reshape(1, width),
        post_ffn_gain.reshape(1, width),
        route_ids,
        route_weight,
        expert_gate,
        expert_up,
        expert_down,
    )


def solution(mesh):
    in_specs = (
        P(("sp", "tp"), None),
        P("sp", "tp"),
        P("tp", None, None),
        P("tp"),
        P(),
        P(),
        P(),
        P(),
        P(("sp", "tp"), None),
        P(("sp", "tp"), None),
        P("sp", None, "tp"),
        P("sp", None, "tp"),
        P("sp", "tp", None),
    )
    out_specs = P(("sp", "tp"), None)
    return jax.shard_map(body, mesh=mesh, in_specs=in_specs, out_specs=out_specs, check_vma=False)
```

profile of v0, /device:TPU:18, one launch (start us, length us, event | category | flops | bytes accessed | tf_op | source)
XLA Modules:
  0.0 137.7 jit_solution(2152588200657202555)
XLA Ops:
  0.0 1.4 %copy.14.route_ids = s32[128,2]{1,0:T(8,128)} copy(s32[128,2]{0,1:T(2,128)} %param.21) | data formatting | bytes 2048 | tf_op args[8]
  1.4 1.4 %copy.15.route_weight = f32[128,2]{1,0:T(8,128)} copy(f32[128,2]{0,1:T(2,128)} %param.22) | data formatting | bytes 2048 | tf_op args[9]
  2.8 133.0 %shard_map.127 = bf16[128,2048]{1,0:T(8,128)(2,1)} custom-call(bf16[128,2048]{1,0:T(8,128)(2,1)} %residual.1, bf16[256,1024]{1,0:T(8,128)(2,1)} %projected.1, bf16[2,512,512]{2,1,0:T(8,128)(2,1)} %group_weight.1, f32[1,1024]{1,0:T(1,128)} %bitcast.7, bf16[2048,2048]{1,0:T(8,128)(2,1)} %out_hbm.1, f32[1,2048]{1,0:T(1,128)} %bitcast.4, f32[1,2048]{1,0:T(1,128)} %bitcast.5, ...), custom_call_target="tpu_custom_call" | custom-call | tf_op jit(solution)/shard_map/pallas_call | solution.py:371
  135.8 1.9 %copy.17 = bf16[128,2048]{1,0:T(8,128)(2,1)} copy(bf16[128,2048]{1,0:T(8,128)(2,1)} %shard_map.127) | data formatting | bytes 1048576
where the time goes:
time: 138 us
  Pallas kernels  133 us (96%)
  local copies, waits for them, and re-layouts  4.7 us (3%)
    pallas_call x1, Pallas kernels, body(): pl.pallas_call(functools.partial(layer_kernel, experts, cap), out_shape=j...  133 us
    unnamed x3, local copies, waits for them, and re-layouts  4.7 us

commit v1 on v0

--- a/solution.py
+++ b/solution.py
@@ -344,6 +344,547 @@
         edge.wait_send()
 
 
+def line_kernel(
+    experts,
+    cap,
+    residual,
+    projected,
+    group_weight,
+    channel_scale,
+    out_hbm,
+    post_mix_gain,
+    pre_ffn_gain,
+    post_ffn_gain,
+    route_ids,
+    route_weight,
+    gate_hbm,
+    up_hbm,
+    down_hbm,
+    result,
+    gate_all,
+    up_all,
+    down_all,
+    out_all,
+    raw,
+    rows,
+    across,
+    active,
+    partial,
+    mirrored,
+    back,
+    halo,
+    scaled,
+    received,
+    mixed,
+    middle,
+    ids,
+    picks,
+    weigh,
+    local_sem,
+    weight_send,
+    weight_recv,
+    front_send,
+    front_recv,
+    ids_send,
+    ids_recv,
+    raw_send,
+    raw_recv,
+    y_send,
+    y_recv,
+    x_send,
+    x_recv,
+    swap_send,
+    swap_recv,
+    back_send,
+    back_recv,
+):
+    place = lax.axis_index("sp")
+    core = lax.axis_index("tp")
+    places = lax.axis_size("sp")
+    planes = places // 4
+    last = planes - 1
+    z, y, x = place // 4, (place // 2) % 2, place % 2
+    half = z // (planes // 2)
+    inward = 1 - 2 * half
+    own = (z + half) % 2
+    partner = (place, 1 - core)
+    quarter = gate_hbm.shape[2]
+    hidden = 2 * quarter
+    share, width = residual.shape
+    tokens, cut = projected.shape
+    lookback = halo.shape[0]
+    block_rows = 4 * cap
+    piece = share // 2
+
+    def spot(s, other_y, other_x):
+        at_z = s + half * (last - 2 * s)
+        at_y = 1 - y if other_y else y
+        at_x = 1 - x if other_x else x
+        return (at_z * 4 + at_y * 2 + at_x, core)
+
+    def remote(source, target, device, first, second):
+        return pltpu.make_async_remote_copy(
+            src_ref=source,
+            dst_ref=target,
+            send_sem=first,
+            recv_sem=second,
+            device_id=device,
+            device_id_type=MESH,
+        )
+
+    weights = [
+        (gate_hbm.at[0], gate_all.at[:, pl.ds(0, quarter)], gate_all.at[:, pl.ds(quarter, quarter)]),
+        (up_hbm.at[0], up_all.at[:, pl.ds(0, quarter)], up_all.at[:, pl.ds(quarter, quarter)]),
+        (down_hbm.at[0], down_all.at[pl.ds(0, quarter)], down_all.at[pl.ds(quarter, quarter)]),
+    ]
+    out_load = pltpu.make_async_copy(out_hbm, out_all, local_sem.at[3])
+    out_load.start()
+    loads = []
+    for i, (source, mine, _) in enumerate(weights):
+        load = pltpu.make_async_copy(source, mine, local_sem.at[i])
+        load.start()
+        loads.append(load)
+
+    barrier = pltpu.get_barrier_semaphore()
+    for step in range(1, places):
+        device = ((place + step) % places, core)
+        pl.semaphore_signal(barrier, inc=1, device_id=device, device_id_type=MESH)
+    pl.semaphore_signal(barrier, inc=1, device_id=partner, device_id_type=MESH)
+    pl.semaphore_wait(barrier, places)
+
+    edge = remote(
+        projected.at[pl.ds(tokens - lookback, lookback)],
+        halo,
+        ((place + 1) % places, core),
+        front_send.at[0],
+        front_recv.at[0],
+    )
+
+    @pl.when(place < places - 1)
+    def _():
+        edge.start()
+
+    ids[own] = jnp.concatenate(
+        [route_ids[...], jnp.zeros((ids.shape[1] - TOP, share), jnp.int32)], 0
+    )
+
+    def id_copies(role):
+        if role == 0:
+            targets = [(1, False, 0), (2, False, 3), (3, False, 3)]
+            targets += [(0, True, 4), (1, True, 4), (2, True, 5), (3, True, 5)]
+        else:
+            targets = [(0, False, 1), (2, False, 2), (3, False, 2)]
+        return [
+            remote(ids.at[role], ids.at[j], spot(s, False, turn), ids_send.at[i], ids_recv.at[j])
+            for i, (s, turn, j) in enumerate(targets)
+        ]
+
+    def expect(target, semaphore):
+        return remote(target, target, partner, local_sem.at[0], semaphore)
+
+    for role in range(2):
+
+        @pl.when(own == role)
+        def _(role=role):
+            for copy in id_copies(role):
+                copy.start()
+
+    for role in range(2):
+
+        @pl.when(own == role)
+        def _(role=role):
+            for j in range(6):
+                if j != role:
+                    expect(ids.at[j], ids_recv.at[j]).wait_recv()
+
+    sub = lax.broadcasted_iota(jnp.int32, (8, share), 0)
+    here_expert = 2 * z + jnp.where(sub == 0, y, 1 - y)
+    at = sub // 2
+    turn = sub % 2
+    home_expert = 2 * (at + half * (last - 2 * at)) + (y + turn - 2 * y * turn)
+    members = []
+    for j in range(6):
+        first, second = ids[j, 0:1, :], ids[j, 1:2, :]
+        named = jnp.logical_or(first == here_expert, second == here_expert)
+        members.append(jnp.where(jnp.logical_and(named, sub < 2), 1.0, 0.0))
+    first, second = route_ids[0:1, :] == home_expert, route_ids[1:2, :] == home_expert
+    members.append(jnp.where(jnp.logical_or(first, second), 1.0, 0.0))
+    factor = jnp.where(first, route_weight[0:1, :], 0.0) + jnp.where(
+        second, route_weight[1:2, :], 0.0
+    )
+    member = jnp.concatenate(members, 0)
+    earlier = jnp.where(
+        lax.broadcasted_iota(jnp.int32, (share, share), 0)
+        < lax.broadcasted_iota(jnp.int32, (share, share), 1),
+        1.0,
+        0.0,
+    ).astype(jnp.bfloat16)
+    rank = jnp.dot(member.astype(jnp.bfloat16), earlier, preferred_element_type=jnp.float32)
+    slot = lax.broadcasted_iota(jnp.int32, (cap, share), 0).astype(jnp.float32)
+    for j in range(6):
+        pair = [
+            jnp.where(rank[8 * j + i : 8 * j + i + 1] == slot, member[8 * j + i : 8 * j + i + 1], 0.0)
+            for i in range(2)
+        ]
+        picks[j] = jnp.concatenate(pair, 0).astype(jnp.bfloat16)
+    for s in range(4):
+        pair = [
+            jnp.where(rank[48 + i : 49 + i] == slot, factor[i : i + 1], 0.0)
+            for i in (2 * s, 2 * s + 1)
+        ]
+        full = jnp.concatenate(pair, 0).T
+        high = full.astype(jnp.bfloat16)
+        weigh[s, 0] = high
+        weigh[s, 1] = (full - high.astype(jnp.float32)).astype(jnp.bfloat16)
+
+    @pl.when(place > 0)
+    def _():
+        edge.wait_recv()
+
+    @pl.when(place == 0)
+    def _():
+        halo[...] = jnp.zeros_like(halo)
+
+    position = (
+        place * tokens + lax.broadcasted_iota(jnp.int32, (tokens, 1), 0) + 1
+    ).astype(jnp.float32)
+    groups_here = group_weight.shape[0]
+    group_width = cut // groups_here
+    for local_group in range(groups_here):
+        low = local_group * group_width
+        own_part = projected[:, low : low + group_width].astype(jnp.float32)
+        current = jnp.concatenate(
+            [halo[:, low : low + group_width].astype(jnp.float32), own_part], 0
+        )
+        group_id = core * groups_here + local_group
+        summed = own_part
+        window_span = jnp.float32(1.0)
+        for level_id in range(GROUPS):
+            current = current + pltpu.roll(current, 2**level_id, 0)
+            hit = group_id == level_id
+            summed = jnp.where(hit, current[lookback:], summed)
+            window_span = jnp.where(hit, jnp.float32(2.0 ** (level_id + 1)), window_span)
+        pooled = (summed / jnp.minimum(position, window_span) - own_part).astype(jnp.bfloat16)
+        grouped = jnp.dot(pooled, group_weight[local_group], preferred_element_type=jnp.float32)
+        scaled[:, low : low + group_width] = (
+            grouped * channel_scale[:, low : low + group_width]
+        ).astype(jnp.bfloat16)
+    there = pl.ds(pl.multiple_of((1 - core) * share, share), share)
+    here = pl.ds(pl.multiple_of(core * share, share), share)
+    exchange = remote(scaled.at[there], received, partner, front_send.at[1], front_recv.at[1])
+    exchange.start()
+    out_load.wait()
+
+    def mix(block, first_row, fresh):
+        def step(t, carry):
+            at = pl.ds(pl.multiple_of(t * WIDE, WIDE), WIDE)
+            value = jnp.dot(
+                block, out_all[pl.ds(first_row, cut), at], preferred_element_type=jnp.float32
+            )
+            mixed[:, at] = value if fresh else mixed[:, at] + value
+            return carry
+
+        lax.fori_loop(0, width // WIDE, step, 0)
+
+    mix(scaled[here], pl.multiple_of(core * cut, cut), True)
+    exchange.wait_recv()
+    gathers = [
+        remote(source, theirs, partner, weight_send.at[i], weight_recv.at[i])
+        for i, (source, _, theirs) in enumerate(weights)
+    ]
+    for copy in gathers:
+        copy.start()
+    mix(received[...], pl.multiple_of((1 - core) * cut, cut), False)
+    rounded = mixed[...].astype(jnp.bfloat16).astype(jnp.float32)
+    kept = residual[...].astype(jnp.float32) + rms_scale(rounded, post_mix_gain[...])
+    middle[...] = kept.astype(jnp.bfloat16)
+    raw[own] = rms_scale(middle[...].astype(jnp.float32), pre_ffn_gain[...]).astype(jnp.bfloat16)
+
+    def program(role):
+        sent = list(id_copies(role))
+        state = {"loaded": False}
+
+        def launch(copy):
+            copy.start()
+            sent.append(copy)
+
+        def raw_out(number, source, target, device, part):
+            span = pl.ds(part * piece, piece)
+            launch(
+                remote(
+                    raw.at[source, span],
+                    raw.at[target, span],
+                    device,
+                    raw_send.at[number, part],
+                    raw_recv.at[target, part],
+                )
+            )
+
+        def raw_in(j, part):
+            span = pl.ds(part * piece, piece)
+            expect(raw.at[j, span], raw_recv.at[j, part]).wait_recv()
+
+        def row_of(j):
+            return j * block_rows if j < 4 else (j - 4) * 3 * block_rows + 2 * cap
+
+        def select(j):
+            low = row_of(j)
+
+            def step(t, carry):
+                at = pl.ds(pl.multiple_of(t * WIDE, WIDE), WIDE)
+                value = jnp.dot(picks[j], raw[j, :, at], preferred_element_type=jnp.float32)
+                value = value.astype(jnp.bfloat16)
+                rows[pl.ds(low, cap), at] = value[:cap]
+                across[j, :, at] = value[cap:]
+                return carry
+
+            lax.fori_loop(0, width // WIDE, step, 0)
+            launch(
+                remote(
+                    across.at[j],
+                    rows.at[pl.ds(low + cap, cap)],
+                    spot(role, True, False),
+                    y_send.at[j],
+                    y_recv.at[j],
+                )
+            )
+
+        def y_in(j):
+            expect(rows.at[pl.ds(row_of(j) + cap, cap)], y_recv.at[j]).wait_recv()
+
+        def x_out(s, side):
+            low = s * block_rows + side * cap
+            number = 2 * (s - 1) + side
+            launch(
+                remote(
+                    rows.at[pl.ds(low, cap)],
+                    rows.at[pl.ds(low + 2 * cap, cap)],
+                    spot(role, False, True),
+                    x_send.at[number],
+                    x_recv.at[number],
+                )
+            )
+
+        def x_in(s, side):
+            low = s * block_rows + (2 + side) * cap
+            expect(rows.at[pl.ds(low, cap)], x_recv.at[2 * (s - 1) + side]).wait_recv()
+
+        def compute(s):
+            base = s * block_rows
+            if not state["loaded"]:
+                for i in range(2):
+                    loads[i].wait()
+                    gathers[i].wait_recv()
+
+            def enter(t, carry):
+                at = pl.ds(pl.multiple_of(t * TILE, TILE), TILE)
+                block = rows[pl.ds(base, block_rows), :]
+                gate = jnp.dot(block, gate_all[:, at], preferred_element_type=jnp.float32)
+                up = jnp.dot(block, up_all[:, at], preferred_element_type=jnp.float32)
+                active[:, at] = (jax.nn.silu(gate) * up).astype(jnp.bfloat16)
+                return carry
+
+            lax.fori_loop(0, hidden // TILE, enter, 0)
+            if not state["loaded"]:
+                loads[2].wait()
+                gathers[2].wait_recv()
+            state["loaded"] = True
+
+            def leave(t, carry):
+                at = pl.ds(pl.multiple_of(t * TILE, TILE), TILE)
+                value = jnp.dot(active[...], down_all[:, at], preferred_element_type=jnp.float32)
+                partial[pl.ds(base, block_rows), at] = value.astype(jnp.bfloat16)
+                return carry
+
+            lax.fori_loop(0, width // TILE, leave, 0)
+
+        def swap(s, side):
+            span = pl.ds(side * cap, cap)
+            launch(
+                remote(
+                    partial.at[pl.ds(s * block_rows + (2 + side) * cap, cap)],
+                    mirrored.at[s, span],
+                    spot(role, False, True),
+                    swap_send.at[s, side],
+                    swap_recv.at[s, side],
+                )
+            )
+
+        def finish(s, side):
+            arrived = mirrored.at[s, pl.ds(side * cap, cap)]
+            expect(arrived, swap_recv.at[s, side]).wait_recv()
+            seen = role if s < 2 else last - role
+            span = pl.ds(s * block_rows + side * cap, cap)
+            total = partial[span].astype(jnp.float32) + arrived[...].astype(jnp.float32)
+            if s == role and side == 0:
+                back[2 * s] = total.astype(jnp.bfloat16)
+                return
+            partial[span] = total.astype(jnp.bfloat16)
+            launch(
+                remote(
+                    partial.at[span],
+                    back.at[2 * seen + side],
+                    spot(s, side == 1, False),
+                    back_send.at[2 * s + side],
+                    back_recv.at[2 * seen + side],
+                )
+            )
+
+        def gather(s, fresh):
+            for side in range(2):
+                if s != role or side == 1:
+                    expect(back.at[2 * s + side], back_recv.at[2 * s + side]).wait_recv()
+            for low in range(0, width, WIDE):
+                block = back[2 * s : 2 * s + 2, :, low : low + WIDE].reshape(2 * cap, WIDE)
+                value = jnp.dot(weigh[s, 0], block, preferred_element_type=jnp.float32)
+                value = value + jnp.dot(weigh[s, 1], block, preferred_element_type=jnp.float32)
+                held = mixed[:, low : low + WIDE]
+                mixed[:, low : low + WIDE] = value if fresh else held + value
+
+        near = spot(1 - role, False, False)
+        twin = spot(role, False, True)
+        if role == 0:
+            for part in range(2):
+                raw_out(0, 0, 0, near, part)
+                raw_out(1, 0, 4, twin, part)
+            select(0)
+            raw_in(4, 0)
+            raw_out(2, 4, 4, near, 0)
+            raw_in(1, 0)
+            raw_in(1, 1)
+            select(1)
+            x_out(1, 0)
+            raw_in(4, 1)
+            raw_out(2, 4, 4, near, 1)
+            select(4)
+            y_in(1)
+            x_out(1, 1)
+            raw_in(2, 0)
+            raw_in(2, 1)
+            select(2)
+            x_out(2, 0)
+            y_in(0)
+            y_in(4)
+            compute(0)
+            y_in(2)
+            x_out(2, 1)
+            x_in(1, 0)
+            x_in(1, 1)
+            compute(1)
+            swap(0, 1)
+            raw_in(3, 0)
+            raw_in(3, 1)
+            select(3)
+            x_in(2, 0)
+            x_in(2, 1)
+            compute(2)
+            swap(2, 0)
+            swap(2, 1)
+            swap(1, 0)
+            finish(0, 1)
+            raw_in(5, 0)
+            raw_in(5, 1)
+            select(5)
+            finish(2, 0)
+            finish(2, 1)
+            y_in(3)
+            y_in(5)
+            compute(3)
+            swap(3, 0)
+            swap(3, 1)
+            swap(1, 1)
+            swap(0, 0)
+            finish(1, 0)
+            finish(3, 0)
+            finish(3, 1)
+            gather(1, True)
+            finish(1, 1)
+            gather(2, False)
+            finish(0, 0)
+            gather(0, False)
+            gather(3, False)
+        else:
+            far = spot(2, False, False)
+            for part in range(2):
+                raw_out(0, 1, 1, near, part)
+                raw_out(1, 1, 2, far, part)
+            select(1)
+            x_out(1, 0)
+            y_in(1)
+            x_out(1, 1)
+            for part in range(2):
+                raw_in(0, part)
+                raw_out(2, 0, 3, far, part)
+                raw_in(2, part)
+                raw_out(3, 2, 2, near, part)
+            select(2)
+            x_out(2, 0)
+            select(0)
+            y_in(2)
+            x_out(2, 1)
+            raw_in(3, 0)
+            raw_out(4, 3, 3, near, 0)
+            raw_in(4, 0)
+            raw_out(5, 4, 5, far, 0)
+            x_in(1, 0)
+            x_in(1, 1)
+            compute(1)
+            swap(1, 1)
+            raw_in(3, 1)
+            raw_out(4, 3, 3, near, 1)
+            raw_in(4, 1)
+            raw_out(5, 4, 5, far, 1)
+            select(3)
+            select(4)
+            x_in(2, 0)
+            x_in(2, 1)
+            compute(2)
+            swap(2, 0)
+            swap(2, 1)
+            for part in range(2):
+                raw_in(5, part)
+                raw_out(6, 5, 5, near, part)
+            select(5)
+            y_in(0)
+            y_in(4)
+            compute(0)
+            swap(0, 0)
+            swap(0, 1)
+            finish(2, 0)
+            finish(2, 1)
+            y_in(3)
+            y_in(5)
+            compute(3)
+            swap(3, 0)
+            swap(3, 1)
+            swap(1, 0)
+            finish(1, 1)
+            finish(0, 0)
+            finish(0, 1)
+            finish(3, 0)
+            finish(3, 1)
+            gather(2, True)
+            finish(1, 0)
+            gather(3, False)
+            gather(1, False)
+            gather(0, False)
+        result[...] = (
+            middle[...].astype(jnp.float32) + rms_scale(mixed[...], post_ffn_gain[...])
+        ).astype(jnp.bfloat16)
+        for copy in sent + gathers + [exchange]:
+            copy.wait_send()
+
+    for role in range(2):
+
+        @pl.when(own == role)
+        def _(role=role):
+            program(role)
+
+    @pl.when(place < places - 1)
+    def _():
+        edge.wait_send()
+
+
 def body(
     residual,
     projected,
@@ -368,6 +909,71 @@
     dma = pltpu.SemaphoreType.DMA
     vmem = pl.BlockSpec(memory_space=pltpu.VMEM)
     hbm = pl.BlockSpec(memory_space=pltpu.HBM)
+    if 4 * 4 == lax.axis_size("sp"):
+        sizes = [
+            (width, 2 * quarter),
+            (width, 2 * quarter),
+            (2 * quarter, width),
+            out_weight.shape,
+            (6, share, width),
+            (2 * experts * cap, width),
+            (6, cap, width),
+            (4 * cap, 2 * quarter),
+            (2 * experts * cap, width),
+            (4, 2 * cap, width),
+            (experts, cap, width),
+            (2**GROUPS, cut),
+            (tokens, cut),
+            (share, cut),
+        ]
+        return pl.pallas_call(
+            functools.partial(line_kernel, experts, cap),
+            out_shape=jax.ShapeDtypeStruct((share, width), kinds),
+            in_specs=[vmem] * 4 + [hbm] + [vmem] * 5 + [hbm] * 3,
+            out_specs=vmem,
+            scratch_shapes=[pltpu.VMEM(size, kinds) for size in sizes]
+            + [
+                pltpu.VMEM((share, width), jnp.float32),
+                pltpu.VMEM((share, width), kinds),
+                pltpu.VMEM((6, 8, share), jnp.int32),
+                pltpu.VMEM((6, 2 * cap, share), kinds),
+                pltpu.VMEM((4, 2, share, 2 * cap), kinds),
+                dma((4,)),
+                dma((3,)),
+                dma((3,)),
+                dma((2,)),
+                dma((2,)),
+                dma((7,)),
+                dma((6,)),
+                dma((7, 2)),
+                dma((6, 2)),
+                dma((6,)),
+                dma((6,)),
+                dma((4,)),
+                dma((4,)),
+                dma((4, 2)),
+                dma((4, 2)),
+                dma((8,)),
+                dma((8,)),
+            ],
+            compiler_params=pltpu.CompilerParams(
+                collective_id=0, has_side_effects=True, vmem_limit_bytes=62 * 1024 * 1024
+            ),
+        )(
+            residual,
+            projected,
+            group_weight,
+            channel_scale.reshape(1, cut),
+            out_weight,
+            post_mix_gain.reshape(1, width),
+            pre_ffn_gain.reshape(1, width),
+            post_ffn_gain.reshape(1, width),
+            route_ids.T,
+            route_weight.T,
+            expert_gate,
+            expert_up,
+            expert_down,
+        )
     return pl.pallas_call(
         functools.partial(layer_kernel, experts, cap),
         out_shape=jax.ShapeDtypeStruct((share, width), kinds),

time: 138 us -> 121 us (0.88)
  the two profiles are of different devices: /device:TPU:18 before, /device:TPU:0 now
where the time goes in v1:
time: 121 us; the launch traced here: 120 us
  Pallas kernels  119 us (98%)
  local copies, waits for them, and re-layouts  1.88 us (2%)
    pallas_call x1, Pallas kernels, body(): pl.pallas_call(functools.partial(line_kernel, experts, cap), out_shape=ja...  119 us

profile of v1, /device:TPU:0, one launch (start us, length us, event | category | flops | bytes accessed | tf_op | source)
XLA Modules:
  0.0 120.4 jit_solution(7565350977064682836)
XLA Ops:
  0.0 118.5 %shard_map.127 = bf16[128,2048]{1,0:T(8,128)(2,1)} custom-call(bf16[128,2048]{1,0:T(8,128)(2,1)} %residual.1, bf16[256,1024]{1,0:T(8,128)(2,1)} %projected.1, bf16[2,512,512]{2,1,0:T(8,128)(2,1)} %group_weight.1, f32[1,1024]{1,0:T(1,128)} %bitcast.9, bf16[2048,2048]{1,0:T(8,128)(2,1)} %out_hbm.1, f32[1,2048]{1,0:T(1,128)} %bitcast.6, f32[1,2048]{1,0:T(1,128)} %bitcast.7, ...), custom_call_target="tpu_custom_call" | custom-call | tf_op jit(solution)/shard_map/pallas_call | solution.py:929
  118.5 1.9 %copy.15 = bf16[128,2048]{1,0:T(8,128)(2,1)} copy(bf16[128,2048]{1,0:T(8,128)(2,1)} %shard_map.127) | data formatting | bytes 1048576

commit v2 on v1

--- a/solution.py
+++ b/solution.py
@@ -415,6 +415,7 @@
     lookback = halo.shape[0]
     block_rows = 4 * cap
     piece = share // 2
+    up_tile = hidden // 2
 
     def spot(s, other_y, other_x):
         at_z = s + half * (last - 2 * s)
@@ -487,6 +488,98 @@
         @pl.when(own == role)
         def _(role=role):
             for copy in id_copies(role):
+                copy.start()
+
+    @pl.when(place > 0)
+    def _():
+        edge.wait_recv()
+
+    @pl.when(place == 0)
+    def _():
+        halo[...] = jnp.zeros_like(halo)
+
+    position = (
+        place * tokens + lax.broadcasted_iota(jnp.int32, (tokens, 1), 0) + 1
+    ).astype(jnp.float32)
+    groups_here = group_weight.shape[0]
+    group_width = cut // groups_here
+    for local_group in range(groups_here):
+        low = local_group * group_width
+        own_part = projected[:, low : low + group_width].astype(jnp.float32)
+        current = jnp.concatenate(
+            [halo[:, low : low + group_width].astype(jnp.float32), own_part], 0
+        )
+        group_id = core * groups_here + local_group
+        summed = own_part
+        window_span = jnp.float32(1.0)
+        for level_id in range(GROUPS):
+            current = current + pltpu.roll(current, 2**level_id, 0)
+            hit = group_id == level_id
+            summed = jnp.where(hit, current[lookback:], summed)
+            window_span = jnp.where(hit, jnp.float32(2.0 ** (level_id + 1)), window_span)
+        pooled = (summed / jnp.minimum(position, window_span) - own_part).astype(jnp.bfloat16)
+        grouped = jnp.dot(pooled, group_weight[local_group], preferred_element_type=jnp.float32)
+        scaled[:, low : low + group_width] = (
+            grouped * channel_scale[:, low : low + group_width]
+        ).astype(jnp.bfloat16)
+    there = pl.ds(pl.multiple_of((1 - core) * share, share), share)
+    here = pl.ds(pl.multiple_of(core * share, share), share)
+    exchange = remote(scaled.at[there], received, partner, front_send.at[1], front_recv.at[1])
+    exchange.start()
+    out_load.wait()
+
+    def mix(block, first_row, fresh):
+        def step(t, carry):
+            at = pl.ds(pl.multiple_of(t * WIDE, WIDE), WIDE)
+            value = jnp.dot(
+                block, out_all[pl.ds(first_row, cut), at], preferred_element_type=jnp.float32
+            )
+            mixed[:, at] = value if fresh else mixed[:, at] + value
+            return carry
+
+        lax.fori_loop(0, width // WIDE, step, 0)
+
+    mix(scaled[here], pl.multiple_of(core * cut, cut), True)
+    exchange.wait_recv()
+    gathers = [
+        remote(source, theirs, partner, weight_send.at[i], weight_recv.at[i])
+        for i, (source, _, theirs) in enumerate(weights)
+    ]
+    for copy in gathers:
+        copy.start()
+    mix(received[...], pl.multiple_of((1 - core) * cut, cut), False)
+    rounded = mixed[...].astype(jnp.bfloat16).astype(jnp.float32)
+    kept = residual[...].astype(jnp.float32) + rms_scale(rounded, post_mix_gain[...])
+    middle[...] = kept.astype(jnp.bfloat16)
+    raw[own] = rms_scale(middle[...].astype(jnp.float32), pre_ffn_gain[...]).astype(jnp.bfloat16)
+
+    def raw_copy(number, source, target, device, part):
+        span = pl.ds(part * piece, piece)
+        return remote(
+            raw.at[source, span],
+            raw.at[target, span],
+            device,
+            raw_send.at[number, part],
+            raw_recv.at[target, part],
+        )
+
+    def first_copies(role):
+        near, twin = spot(1 - role, False, False), spot(role, False, True)
+        copies = []
+        for part in range(2):
+            if role == 0:
+                copies.append(raw_copy(0, 0, 0, near, part))
+                copies.append(raw_copy(1, 0, 4, twin, part))
+            else:
+                copies.append(raw_copy(0, 1, 1, near, part))
+                copies.append(raw_copy(1, 1, 2, spot(2, False, False), part))
+        return copies
+
+    for role in range(2):
+
+        @pl.when(own == role)
+        def _(role=role):
+            for copy in first_copies(role):
                 copy.start()
 
     for role in range(2):
@@ -537,88 +630,16 @@
         weigh[s, 0] = high
         weigh[s, 1] = (full - high.astype(jnp.float32)).astype(jnp.bfloat16)
 
-    @pl.when(place > 0)
-    def _():
-        edge.wait_recv()
-
-    @pl.when(place == 0)
-    def _():
-        halo[...] = jnp.zeros_like(halo)
-
-    position = (
-        place * tokens + lax.broadcasted_iota(jnp.int32, (tokens, 1), 0) + 1
-    ).astype(jnp.float32)
-    groups_here = group_weight.shape[0]
-    group_width = cut // groups_here
-    for local_group in range(groups_here):
-        low = local_group * group_width
-        own_part = projected[:, low : low + group_width].astype(jnp.float32)
-        current = jnp.concatenate(
-            [halo[:, low : low + group_width].astype(jnp.float32), own_part], 0
-        )
-        group_id = core * groups_here + local_group
-        summed = own_part
-        window_span = jnp.float32(1.0)
-        for level_id in range(GROUPS):
-            current = current + pltpu.roll(current, 2**level_id, 0)
-            hit = group_id == level_id
-            summed = jnp.where(hit, current[lookback:], summed)
-            window_span = jnp.where(hit, jnp.float32(2.0 ** (level_id + 1)), window_span)
-        pooled = (summed / jnp.minimum(position, window_span) - own_part).astype(jnp.bfloat16)
-        grouped = jnp.dot(pooled, group_weight[local_group], preferred_element_type=jnp.float32)
-        scaled[:, low : low + group_width] = (
-            grouped * channel_scale[:, low : low + group_width]
-        ).astype(jnp.bfloat16)
-    there = pl.ds(pl.multiple_of((1 - core) * share, share), share)
-    here = pl.ds(pl.multiple_of(core * share, share), share)
-    exchange = remote(scaled.at[there], received, partner, front_send.at[1], front_recv.at[1])
-    exchange.start()
-    out_load.wait()
-
-    def mix(block, first_row, fresh):
-        def step(t, carry):
-            at = pl.ds(pl.multiple_of(t * WIDE, WIDE), WIDE)
-            value = jnp.dot(
-                block, out_all[pl.ds(first_row, cut), at], preferred_element_type=jnp.float32
-            )
-            mixed[:, at] = value if fresh else mixed[:, at] + value
-            return carry
-
-        lax.fori_loop(0, width // WIDE, step, 0)
-
-    mix(scaled[here], pl.multiple_of(core * cut, cut), True)
-    exchange.wait_recv()
-    gathers = [
-        remote(source, theirs, partner, weight_send.at[i], weight_recv.at[i])
-        for i, (source, _, theirs) in enumerate(weights)
-    ]
-    for copy in gathers:
-        copy.start()
-    mix(received[...], pl.multiple_of((1 - core) * cut, cut), False)
-    rounded = mixed[...].astype(jnp.bfloat16).astype(jnp.float32)
-    kept = residual[...].astype(jnp.float32) + rms_scale(rounded, post_mix_gain[...])
-    middle[...] = kept.astype(jnp.bfloat16)
-    raw[own] = rms_scale(middle[...].astype(jnp.float32), pre_ffn_gain[...]).astype(jnp.bfloat16)
-
     def program(role):
-        sent = list(id_copies(role))
-        state = {"loaded": False}
+        sent = id_copies(role) + first_copies(role)
+        state = {"entered": False, "left": False, "summed": False}
 
         def launch(copy):
             copy.start()
             sent.append(copy)
 
-        def raw_out(number, source, target, device, part):
-            span = pl.ds(part * piece, piece)
-            launch(
-                remote(
-                    raw.at[source, span],
-                    raw.at[target, span],
-                    device,
-                    raw_send.at[number, part],
-                    raw_recv.at[target, part],
-                )
-            )
+        def raw_out(*hop):
+            launch(raw_copy(*hop))
 
         def raw_in(j, part):
             span = pl.ds(part * piece, piece)
@@ -669,34 +690,38 @@
             low = s * block_rows + (2 + side) * cap
             expect(rows.at[pl.ds(low, cap)], x_recv.at[2 * (s - 1) + side]).wait_recv()
 
-        def compute(s):
+        def enter(s):
             base = s * block_rows
-            if not state["loaded"]:
+            if not state["entered"]:
                 for i in range(2):
                     loads[i].wait()
                     gathers[i].wait_recv()
-
-            def enter(t, carry):
-                at = pl.ds(pl.multiple_of(t * TILE, TILE), TILE)
+            state["entered"] = True
+
+            def step(t, carry):
+                at = pl.ds(pl.multiple_of(t * up_tile, up_tile), up_tile)
                 block = rows[pl.ds(base, block_rows), :]
                 gate = jnp.dot(block, gate_all[:, at], preferred_element_type=jnp.float32)
                 up = jnp.dot(block, up_all[:, at], preferred_element_type=jnp.float32)
                 active[:, at] = (jax.nn.silu(gate) * up).astype(jnp.bfloat16)
                 return carry
 
-            lax.fori_loop(0, hidden // TILE, enter, 0)
-            if not state["loaded"]:
+            lax.fori_loop(0, hidden // up_tile, step, 0)
+
+        def leave(s):
+            base = s * block_rows
+            if not state["left"]:
                 loads[2].wait()
                 gathers[2].wait_recv()
-            state["loaded"] = True
-
-            def leave(t, carry):
-                at = pl.ds(pl.multiple_of(t * TILE, TILE), TILE)
+            state["left"] = True
+
+            def step(t, carry):
+                at = pl.ds(pl.multiple_of(t * WIDE, WIDE), WIDE)
                 value = jnp.dot(active[...], down_all[:, at], preferred_element_type=jnp.float32)
                 partial[pl.ds(base, block_rows), at] = value.astype(jnp.bfloat16)
                 return carry
 
-            lax.fori_loop(0, width // TILE, leave, 0)
+            lax.fori_loop(0, width // WIDE, step, 0)
 
         def swap(s, side):
             span = pl.ds(side * cap, cap)
@@ -730,7 +755,9 @@
                 )
             )
 
-        def gather(s, fresh):
+        def gather(s):
+            fresh = not state["summed"]
+            state["summed"] = True
             for side in range(2):
                 if s != role or side == 1:
                     expect(back.at[2 * s + side], back_recv.at[2 * s + side]).wait_recv()
@@ -742,132 +769,137 @@
                 mixed[:, low : low + WIDE] = value if fresh else held + value
 
         near = spot(1 - role, False, False)
-        twin = spot(role, False, True)
         if role == 0:
-            for part in range(2):
-                raw_out(0, 0, 0, near, part)
-                raw_out(1, 0, 4, twin, part)
             select(0)
             raw_in(4, 0)
+            raw_in(4, 1)
+            raw_in(1, 1)
             raw_out(2, 4, 4, near, 0)
             raw_in(1, 0)
-            raw_in(1, 1)
             select(1)
             x_out(1, 0)
-            raw_in(4, 1)
+            raw_in(2, 0)
+            y_in(0)
+            select(4)
             raw_out(2, 4, 4, near, 1)
-            select(4)
             y_in(1)
             x_out(1, 1)
-            raw_in(2, 0)
             raw_in(2, 1)
             select(2)
             x_out(2, 0)
-            y_in(0)
             y_in(4)
-            compute(0)
+            enter(0)
+            leave(0)
             y_in(2)
             x_out(2, 1)
+            swap(0, 1)
+            x_in(1, 1)
             x_in(1, 0)
-            x_in(1, 1)
-            compute(1)
-            swap(0, 1)
+            enter(1)
+            leave(1)
             raw_in(3, 0)
             raw_in(3, 1)
             select(3)
+            x_in(2, 1)
+            swap(1, 1)
             x_in(2, 0)
-            x_in(2, 1)
-            compute(2)
+            enter(2)
+            leave(2)
             swap(2, 0)
+            finish(1, 1)
+            raw_in(5, 1)
+            raw_in(5, 0)
+            select(5)
             swap(2, 1)
+            y_in(3)
+            finish(2, 0)
             swap(1, 0)
+            finish(2, 1)
+            swap(0, 0)
+            y_in(5)
+            enter(3)
+            leave(3)
+            swap(3, 0)
             finish(0, 1)
-            raw_in(5, 0)
-            raw_in(5, 1)
-            select(5)
-            finish(2, 0)
-            finish(2, 1)
-            y_in(3)
-            y_in(5)
-            compute(3)
-            swap(3, 0)
             swap(3, 1)
-            swap(1, 1)
-            swap(0, 0)
+            gather(1)
             finish(1, 0)
             finish(3, 0)
             finish(3, 1)
-            gather(1, True)
-            finish(1, 1)
-            gather(2, False)
             finish(0, 0)
-            gather(0, False)
-            gather(3, False)
+            gather(2)
+            gather(0)
+            gather(3)
         else:
             far = spot(2, False, False)
-            for part in range(2):
-                raw_out(0, 1, 1, near, part)
-                raw_out(1, 1, 2, far, part)
             select(1)
             x_out(1, 0)
+            raw_in(2, 0)
             y_in(1)
+            raw_out(3, 2, 2, near, 0)
             x_out(1, 1)
-            for part in range(2):
-                raw_in(0, part)
-                raw_out(2, 0, 3, far, part)
-                raw_in(2, part)
-                raw_out(3, 2, 2, near, part)
+            raw_in(0, 0)
+            raw_in(0, 1)
+            raw_in(2, 1)
+            raw_out(2, 0, 3, far, 0)
+            raw_out(3, 2, 2, near, 1)
             select(2)
             x_out(2, 0)
+            raw_out(2, 0, 3, far, 1)
+            x_in(1, 0)
             select(0)
+            x_in(1, 1)
             y_in(2)
             x_out(2, 1)
-            raw_in(3, 0)
-            raw_out(4, 3, 3, near, 0)
             raw_in(4, 0)
             raw_out(5, 4, 5, far, 0)
-            x_in(1, 0)
-            x_in(1, 1)
-            compute(1)
-            swap(1, 1)
+            enter(1)
+            leave(1)
+            raw_in(3, 0)
             raw_in(3, 1)
+            raw_in(4, 1)
             raw_out(4, 3, 3, near, 1)
-            raw_in(4, 1)
             raw_out(5, 4, 5, far, 1)
-            select(3)
+            y_in(0)
             select(4)
+            raw_out(4, 3, 3, near, 0)
+            swap(1, 0)
             x_in(2, 0)
             x_in(2, 1)
-            compute(2)
+            enter(2)
+            leave(2)
+            raw_in(5, 0)
             swap(2, 0)
+            raw_in(5, 1)
+            finish(1, 0)
+            select(3)
             swap(2, 1)
-            for part in range(2):
-                raw_in(5, part)
-                raw_out(6, 5, 5, near, part)
+            y_in(4)
             select(5)
-            y_in(0)
-            y_in(4)
-            compute(0)
-            swap(0, 0)
+            raw_out(6, 5, 5, near, 0)
+            enter(0)
+            leave(0)
             swap(0, 1)
             finish(2, 0)
+            swap(0, 0)
+            y_in(3)
+            raw_out(6, 5, 5, near, 1)
             finish(2, 1)
-            y_in(3)
             y_in(5)
-            compute(3)
+            enter(3)
+            leave(3)
+            finish(0, 1)
+            swap(3, 1)
             swap(3, 0)
-            swap(3, 1)
-            swap(1, 0)
+            finish(0, 0)
+            swap(1, 1)
+            gather(2)
+            finish(3, 1)
+            finish(3, 0)
             finish(1, 1)
-            finish(0, 0)
-            finish(0, 1)
-            finish(3, 0)
-            finish(3, 1)
-            gather(2, True)
-            finish(1, 0)
-            gather(3, False)
-            gather(1, False)
-            gather(0, False)
+            gather(1)
+            gather(3)
+            gather(0)
         result[...] = (
             middle[...].astype(jnp.float32) + rms_scale(mixed[...], post_ffn_gain[...])
         ).astype(jnp.bfloat16)

time: 121 us -> 114 us (0.942)
  Pallas kernels: 119 us -> 112 us
    pallas_call x1, Pallas kernels: 119 us -> 112 us  [body(): pl.pallas_call(functools.partial(line_kernel, experts, cap), out_shape=ja...]
where the time goes in v2:
time: 114 us
  Pallas kernels  112 us (98%)
  local copies, waits for them, and re-layouts  1.88 us (2%)
    pallas_call x1, Pallas kernels, body(): pl.pallas_call(functools.partial(line_kernel, experts, cap), out_shape=ja...  112 us

profile of v2, /device:TPU:0, one launch (start us, length us, event | category | flops | bytes accessed | tf_op | source)
XLA Modules:
  0.0 114.0 jit_solution(8183496817910740469)
XLA Ops:
  0.0 112.2 %shard_map.127 = bf16[128,2048]{1,0:T(8,128)(2,1)} custom-call(bf16[128,2048]{1,0:T(8,128)(2,1)} %residual.1, bf16[256,1024]{1,0:T(8,128)(2,1)} %projected.1, bf16[2,512,512]{2,1,0:T(8,128)(2,1)} %group_weight.1, f32[1,1024]{1,0:T(1,128)} %bitcast.9, bf16[2048,2048]{1,0:T(8,128)(2,1)} %out_hbm.1, f32[1,2048]{1,0:T(1,128)} %bitcast.6, f32[1,2048]{1,0:T(1,128)} %bitcast.7, ...), custom_call_target="tpu_custom_call" | custom-call | tf_op jit(solution)/shard_map/pallas_call | solution.py:961
  112.2 1.9 %copy.15 = bf16[128,2048]{1,0:T(8,128)(2,1)} copy(bf16[128,2048]{1,0:T(8,128)(2,1)} %shard_map.127) | data formatting | bytes 1048576

commit v3 on v2

--- a/solution.py
+++ b/solution.py
@@ -415,6 +415,7 @@
     lookback = halo.shape[0]
     block_rows = 4 * cap
     piece = share // 2
+    finer = cap // 2
     up_tile = hidden // 2
 
     def spot(s, other_y, other_x):
@@ -690,8 +691,9 @@
             low = s * block_rows + (2 + side) * cap
             expect(rows.at[pl.ds(low, cap)], x_recv.at[2 * (s - 1) + side]).wait_recv()
 
-        def enter(s):
-            base = s * block_rows
+        def enter(s, part=None):
+            base = s * block_rows + (part or 0) * 2 * cap
+            count = block_rows if part is None else 2 * cap
             if not state["entered"]:
                 for i in range(2):
                     loads[i].wait()
@@ -700,16 +702,17 @@
 
             def step(t, carry):
                 at = pl.ds(pl.multiple_of(t * up_tile, up_tile), up_tile)
-                block = rows[pl.ds(base, block_rows), :]
+                block = rows[pl.ds(base, count), :]
                 gate = jnp.dot(block, gate_all[:, at], preferred_element_type=jnp.float32)
                 up = jnp.dot(block, up_all[:, at], preferred_element_type=jnp.float32)
-                active[:, at] = (jax.nn.silu(gate) * up).astype(jnp.bfloat16)
+                active[:count, at] = (jax.nn.silu(gate) * up).astype(jnp.bfloat16)
                 return carry
 
             lax.fori_loop(0, hidden // up_tile, step, 0)
 
-        def leave(s):
-            base = s * block_rows
+        def leave(s, part=None):
+            base = s * block_rows + (part or 0) * 2 * cap
+            count = block_rows if part is None else 2 * cap
             if not state["left"]:
                 loads[2].wait()
                 gathers[2].wait_recv()
@@ -717,50 +720,55 @@
 
             def step(t, carry):
                 at = pl.ds(pl.multiple_of(t * WIDE, WIDE), WIDE)
-                value = jnp.dot(active[...], down_all[:, at], preferred_element_type=jnp.float32)
-                partial[pl.ds(base, block_rows), at] = value.astype(jnp.bfloat16)
+                value = jnp.dot(active[:count, :], down_all[:, at], preferred_element_type=jnp.float32)
+                partial[pl.ds(base, count), at] = value.astype(jnp.bfloat16)
                 return carry
 
             lax.fori_loop(0, width // WIDE, step, 0)
 
         def swap(s, side):
-            span = pl.ds(side * cap, cap)
-            launch(
-                remote(
-                    partial.at[pl.ds(s * block_rows + (2 + side) * cap, cap)],
-                    mirrored.at[s, span],
-                    spot(role, False, True),
-                    swap_send.at[s, side],
-                    swap_recv.at[s, side],
+            for part in range(2):
+                low = side * cap + part * finer
+                launch(
+                    remote(
+                        partial.at[pl.ds(s * block_rows + 2 * cap + low, finer)],
+                        mirrored.at[s, pl.ds(low, finer)],
+                        spot(role, False, True),
+                        swap_send.at[s, side, part],
+                        swap_recv.at[s, side, part],
+                    )
                 )
-            )
 
         def finish(s, side):
-            arrived = mirrored.at[s, pl.ds(side * cap, cap)]
-            expect(arrived, swap_recv.at[s, side]).wait_recv()
             seen = role if s < 2 else last - role
-            span = pl.ds(s * block_rows + side * cap, cap)
-            total = partial[span].astype(jnp.float32) + arrived[...].astype(jnp.float32)
-            if s == role and side == 0:
-                back[2 * s] = total.astype(jnp.bfloat16)
-                return
-            partial[span] = total.astype(jnp.bfloat16)
-            launch(
-                remote(
-                    partial.at[span],
-                    back.at[2 * seen + side],
-                    spot(s, side == 1, False),
-                    back_send.at[2 * s + side],
-                    back_recv.at[2 * seen + side],
+            for part in range(2):
+                low = side * cap + part * finer
+                arrived = mirrored.at[s, pl.ds(low, finer)]
+                expect(arrived, swap_recv.at[s, side, part]).wait_recv()
+                span = pl.ds(s * block_rows + low, finer)
+                total = partial[span].astype(jnp.float32) + arrived[...].astype(jnp.float32)
+                if s == role and side == 0:
+                    back[2 * s, pl.ds(part * finer, finer)] = total.astype(jnp.bfloat16)
+                    continue
+                partial[span] = total.astype(jnp.bfloat16)
+                launch(
+                    remote(
+                        partial.at[span],
+                        back.at[2 * seen + side, pl.ds(part * finer, finer)],
+                        spot(s, side == 1, False),
+                        back_send.at[2 * s + side, part],
+                        back_recv.at[2 * seen + side, part],
+                    )
                 )
-            )
 
         def gather(s):
             fresh = not state["summed"]
             state["summed"] = True
             for side in range(2):
                 if s != role or side == 1:
-                    expect(back.at[2 * s + side], back_recv.at[2 * s + side]).wait_recv()
+                    for part in range(2):
+                        piece_in = back.at[2 * s + side, pl.ds(part * finer, finer)]
+                        expect(piece_in, back_recv.at[2 * s + side, part]).wait_recv()
             for low in range(0, width, WIDE):
                 block = back[2 * s : 2 * s + 2, :, low : low + WIDE].reshape(2 * cap, WIDE)
                 value = jnp.dot(weigh[s, 0], block, preferred_element_type=jnp.float32)
@@ -772,133 +780,135 @@
         if role == 0:
             select(0)
             raw_in(4, 0)
-            raw_in(4, 1)
-            raw_in(1, 1)
             raw_out(2, 4, 4, near, 0)
             raw_in(1, 0)
+            raw_in(1, 1)
             select(1)
             x_out(1, 0)
-            raw_in(2, 0)
-            y_in(0)
+            raw_in(4, 1)
+            raw_out(2, 4, 4, near, 1)
             select(4)
-            raw_out(2, 4, 4, near, 1)
             y_in(1)
             x_out(1, 1)
+            raw_in(2, 0)
             raw_in(2, 1)
             select(2)
             x_out(2, 0)
+            y_in(0)
             y_in(4)
             enter(0)
-            leave(0)
             y_in(2)
             x_out(2, 1)
+            leave(0)
             swap(0, 1)
+            x_in(1, 0)
             x_in(1, 1)
-            x_in(1, 0)
             enter(1)
-            leave(1)
             raw_in(3, 0)
             raw_in(3, 1)
             select(3)
-            x_in(2, 1)
+            leave(1)
             swap(1, 1)
             x_in(2, 0)
+            x_in(2, 1)
             enter(2)
+            raw_in(5, 0)
+            raw_in(5, 1)
+            select(5)
             leave(2)
+            swap(2, 1)
             swap(2, 0)
+            y_in(3)
+            enter(3, 0)
+            leave(3, 0)
+            finish(2, 1)
+            y_in(5)
+            enter(3, 1)
+            leave(3, 1)
+            swap(3, 1)
+            swap(3, 0)
+            swap(1, 0)
+            swap(0, 0)
+            finish(2, 0)
             finish(1, 1)
-            raw_in(5, 1)
-            raw_in(5, 0)
-            select(5)
-            swap(2, 1)
-            y_in(3)
-            finish(2, 0)
-            swap(1, 0)
-            finish(2, 1)
-            swap(0, 0)
-            y_in(5)
-            enter(3)
-            leave(3)
-            swap(3, 0)
             finish(0, 1)
-            swap(3, 1)
+            finish(3, 1)
+            finish(3, 0)
+            finish(1, 0)
             gather(1)
-            finish(1, 0)
-            finish(3, 0)
-            finish(3, 1)
+            gather(2)
             finish(0, 0)
-            gather(2)
             gather(0)
             gather(3)
         else:
             far = spot(2, False, False)
             select(1)
             x_out(1, 0)
+            raw_in(0, 0)
+            raw_out(2, 0, 3, far, 0)
             raw_in(2, 0)
+            raw_out(3, 2, 2, near, 0)
             y_in(1)
-            raw_out(3, 2, 2, near, 0)
             x_out(1, 1)
-            raw_in(0, 0)
             raw_in(0, 1)
+            raw_out(2, 0, 3, far, 1)
             raw_in(2, 1)
-            raw_out(2, 0, 3, far, 0)
             raw_out(3, 2, 2, near, 1)
             select(2)
             x_out(2, 0)
-            raw_out(2, 0, 3, far, 1)
+            select(0)
             x_in(1, 0)
-            select(0)
             x_in(1, 1)
             y_in(2)
             x_out(2, 1)
+            enter(1)
+            raw_in(3, 0)
+            raw_out(4, 3, 3, near, 0)
             raw_in(4, 0)
             raw_out(5, 4, 5, far, 0)
-            enter(1)
             leave(1)
-            raw_in(3, 0)
             raw_in(3, 1)
+            raw_out(4, 3, 3, near, 1)
             raw_in(4, 1)
-            raw_out(4, 3, 3, near, 1)
             raw_out(5, 4, 5, far, 1)
-            y_in(0)
+            swap(1, 0)
             select(4)
-            raw_out(4, 3, 3, near, 0)
-            swap(1, 0)
+            select(3)
             x_in(2, 0)
             x_in(2, 1)
             enter(2)
+            raw_in(5, 0)
+            raw_out(6, 5, 5, near, 0)
             leave(2)
-            raw_in(5, 0)
             swap(2, 0)
+            swap(2, 1)
             raw_in(5, 1)
+            raw_out(6, 5, 5, near, 1)
+            select(5)
             finish(1, 0)
-            select(3)
-            swap(2, 1)
+            y_in(0)
             y_in(4)
-            select(5)
-            raw_out(6, 5, 5, near, 0)
             enter(0)
+            finish(2, 0)
             leave(0)
             swap(0, 1)
-            finish(2, 0)
             swap(0, 0)
+            finish(2, 1)
             y_in(3)
-            raw_out(6, 5, 5, near, 1)
-            finish(2, 1)
             y_in(5)
             enter(3)
+            finish(0, 1)
             leave(3)
-            finish(0, 1)
             swap(3, 1)
             swap(3, 0)
+            swap(1, 1)
             finish(0, 0)
-            swap(1, 1)
             gather(2)
             finish(3, 1)
             finish(3, 0)
             finish(1, 1)
+            gather(3)
             gather(1)
-            gather(3)
             gather(0)
         result[...] = (
             middle[...].astype(jnp.float32) + rms_scale(mixed[...], post_ffn_gain[...])
@@ -983,10 +993,10 @@
                 dma((6,)),
                 dma((4,)),
                 dma((4,)),
-                dma((4, 2)),
-                dma((4, 2)),
-                dma((8,)),
-                dma((8,)),
+                dma((4, 2, 2)),
+                dma((4, 2, 2)),
+                dma((8, 2)),
+                dma((8, 2)),
             ],
             compiler_params=pltpu.CompilerParams(
                 collective_id=0, has_side_effects=True, vmem_limit_bytes=62 * 1024 * 1024

time: 114 us -> 112 us (0.982)
  Pallas kernels: 112 us -> 110 us
    pallas_call x1, Pallas kernels: 112 us -> 110 us  [body(): pl.pallas_call(functools.partial(line_kernel, experts, cap), out_shape=ja...]
where the time goes in v3:
time: 112 us
  Pallas kernels  110 us (98%)
  local copies, waits for them, and re-layouts  1.88 us (2%)
    pallas_call x1, Pallas kernels, body(): pl.pallas_call(functools.partial(line_kernel, experts, cap), out_shape=ja...  110 us

profile of v3, /device:TPU:0, one launch (start us, length us, event | category | flops | bytes accessed | tf_op | source)
XLA Modules:
  0.0 112.1 jit_solution(5784036154567318160)
XLA Ops:
  0.0 110.2 %shard_map.127 = bf16[128,2048]{1,0:T(8,128)(2,1)} custom-call(bf16[128,2048]{1,0:T(8,128)(2,1)} %residual.1, bf16[256,1024]{1,0:T(8,128)(2,1)} %projected.1, bf16[2,512,512]{2,1,0:T(8,128)(2,1)} %group_weight.1, f32[1,1024]{1,0:T(1,128)} %bitcast.9, bf16[2048,2048]{1,0:T(8,128)(2,1)} %out_hbm.1, f32[1,2048]{1,0:T(1,128)} %bitcast.6, f32[1,2048]{1,0:T(1,128)} %bitcast.7, ...), custom_call_target="tpu_custom_call" | custom-call | tf_op jit(solution)/shard_map/pallas_call | solution.py:971
  110.2 1.9 %copy.15 = bf16[128,2048]{1,0:T(8,128)(2,1)} copy(bf16[128,2048]{1,0:T(8,128)(2,1)} %shard_map.127) | data formatting | bytes 1048576
